TPU v7x, 32 devices: a whole 2x2x4 slice. The times are simulated.
32 devices in a mesh: grp: 2 (over x), kv: 4 (over z), tp: 4 (over y, core).
Axes of the slice: x: 2, y: 2, z: 4, core: 2. Of those that a mesh axis runs over, the one named last changes fastest.
Arguments:
- tokens: bfloat16 [16, 4096], P('grp', 'tp'), parts along dimension 0, may hold values from -50 to 50
- pre_gain: float32 [4096], P('tp'), may hold values from 0.1 to 1.9
- gate_first: bfloat16 [4096, 11264], P('tp', 'kv'), may hold values from -0.09375 to 0.09375
- up_first: bfloat16 [4096, 11264], P('tp', 'kv'), may hold values from -0.09375 to 0.09375
- down_first: bfloat16 [11264, 4096], P('kv', 'tp'), may hold values from -0.0546875 to 0.0546875
- mix_gain: float32 [4096], P('tp'), may hold values from 0.1 to 1.9
- query_w: bfloat16 [4096, 4096], P('tp', 'kv'), may hold values from -0.09375 to 0.09375
- key_w: bfloat16 [4096, 4096], P('tp', 'kv'), may hold values from -0.09375 to 0.09375
- value_w: bfloat16 [4096, 4096], P('tp', 'kv'), may hold values from -0.09375 to 0.09375
- forget_w: bfloat16 [4096, 32], P('tp'), may hold values from -0.09375 to 0.09375
- key_cache: bfloat16 [16, 1024, 4096], P('grp', 'tp', 'kv'), parts along dimension 0, may hold values from -800 to 800
- value_cache: bfloat16 [16, 1024, 4096], P('grp', 'tp', 'kv'), parts along dimension 0, may hold values from -6 to 6
- gate_cache: float32 [16, 32, 1024], P('grp', 'kv', 'tp'), parts along dimension 0, may hold values from -130 to 0, as said below
- lengths: int32 [16], P('grp'), parts along dimension 0, may hold values from 64 to 1024, as said below
- out_w: bfloat16 [4096, 4096], P('kv', 'tp'), may hold values from -0.09375 to 0.09375
- post_gain: float32 [4096], P('tp'), may hold values from 0.1 to 1.9
- gate_second: bfloat16 [4096, 11264], P('tp', 'kv'), may hold values from -0.09375 to 0.09375
- up_second: bfloat16 [4096, 11264], P('tp', 'kv'), may hold values from -0.09375 to 0.09375
- down_second: bfloat16 [11264, 4096], P('kv', 'tp'), may hold values from -0.0546875 to 0.0546875
Outputs:
- out: bfloat16 [16, 4096], P('grp', 'tp'), parts along dimension 0
There are 2 independent parts, one for each index of `grp`. A program takes and returns all parts, laid end to end along the dimension named above; an argument that names none is the same for every part. Nothing has to cross between parts.
Inputs may be any that keep to these rules, and one draw needn't show every extreme that they name: `lengths`: each sequence's count of live cache positions; one sequence has all 1024 in every draw. `gate_cache`: at a live position p of sequence b, the sum of the log forget values of positions p + 1 to lengths[b] - 1 (zero at the last live position); never positive; zero beyond the live positions.
All inputs are finite; a program needn't handle non-finite values.
Results may differ from a plain program's by a relative error of at most 0.015.
Values may be sent and summed in bfloat16 or wider, within the bound.
A program may use at most 128 MiB of HBM per device.

v0:
```python
import jax
import jax.numpy as jnp
from jax import lax
from jax.sharding import PartitionSpec as P

D = 4096
HEAD_DIM = 128
EPSILON = 1e-06
MASKED = -1e30


def half_step(tok_rows, gain_part, w_gate, w_up, w_down):
    widened = tok_rows.astype(jnp.float32)
    squares = jnp.sum(widened * widened, axis=1)
    weighted = (widened * gain_part).astype(jnp.bfloat16)
    gate_part = jnp.dot(weighted, w_gate, preferred_element_type=jnp.float32)
    up_part = jnp.dot(weighted, w_up, preferred_element_type=jnp.float32)
    gate_sum, up_sum, sq_total = (
        lax.psum(gate_part.astype(jnp.bfloat16), "tp").astype(jnp.float32),
        lax.psum(up_part.astype(jnp.bfloat16), "tp").astype(jnp.float32),
        lax.psum(squares.astype(jnp.bfloat16), "tp").astype(jnp.float32),
    )
    norm_scale = lax.rsqrt(sq_total / D + EPSILON)[:, None]
    hidden = (jax.nn.silu(norm_scale * gate_sum) * (norm_scale * up_sum)).astype(jnp.bfloat16)
    down_part = jnp.dot(hidden, w_down, preferred_element_type=jnp.float32)
    down_sum = lax.psum(down_part, "kv")
    return (widened + 0.5 * down_sum).astype(jnp.bfloat16)


def absorb_parts(running, shard_part):
    run_top, run_mass, run_sum = running
    piece_top, masses, piece_sum = shard_part
    new_top = jnp.maximum(run_top, jnp.max(piece_top, axis=0))
    rescale = jnp.exp(run_top - new_top)
    factors = jnp.exp(piece_top - new_top[None])
    run_mass = run_mass * rescale + jnp.sum(masses * factors, axis=0)
    run_sum = run_sum * rescale[:, :, None] + jnp.sum(
        piece_sum.astype(jnp.float32) * factors[:, :, :, None], axis=0
    )
    return (new_top, run_mass, run_sum)


def attention(
    tok_rows,
    mix_gain,
    query_w,
    key_w,
    value_w,
    forget_w,
    key_cache,
    value_cache,
    gate_cache,
    lengths,
):
    widened = tok_rows.astype(jnp.float32)
    squares = jnp.sum(widened * widened, axis=1)
    weighted = (widened * mix_gain).astype(jnp.bfloat16)
    query_part = jnp.dot(weighted, query_w, preferred_element_type=jnp.float32)
    key_part = jnp.dot(weighted, key_w, preferred_element_type=jnp.float32)
    value_part = jnp.dot(weighted, value_w, preferred_element_type=jnp.float32)
    forget_part = jnp.dot(weighted, forget_w, preferred_element_type=jnp.float32)
    query_sum, key_sum, value_sum, forget_sum, sq_total = lax.psum(
        (query_part, key_part, value_part, forget_part, squares), "tp"
    )
    norm_scale = lax.rsqrt(sq_total / D + EPSILON)[:, None]
    query = (norm_scale * query_sum).astype(jnp.bfloat16)
    key_new = (norm_scale * key_sum).astype(jnp.bfloat16)
    value_new = (norm_scale * value_sum).astype(jnp.bfloat16)
    batch_rows = tok_rows.shape[0]
    heads_here = query.shape[1] // HEAD_DIM
    head_start = lax.axis_index("kv") * heads_here
    log_forget = jax.nn.log_sigmoid(
        norm_scale * lax.dynamic_slice_in_dim(forget_sum, head_start, heads_here, 1)
    )
    cache_span = key_cache.shape[1]
    query_heads = query.reshape(batch_rows, heads_here, HEAD_DIM)
    key_block = key_cache.reshape(batch_rows, cache_span, heads_here, HEAD_DIM)
    value_block = value_cache.reshape(batch_rows, cache_span, heads_here, HEAD_DIM)
    scores = jnp.einsum(
        "bhd,bphd->bhp", query_heads, key_block, preferred_element_type=jnp.float32
    ) * HEAD_DIM ** (-0.5)
    scores = scores + gate_cache + log_forget[:, :, None]
    slot_positions = lax.axis_index("tp") * cache_span + lax.iota(jnp.int32, cache_span)
    is_live = slot_positions[None, None, :] < lengths[:, None, None]
    local_top = jnp.max(jnp.where(is_live, scores, MASKED), axis=2)
    local_probs = jnp.where(is_live, jnp.exp(scores - local_top[:, :, None]), 0.0)
    local_mass = jnp.sum(local_probs, axis=2)
    local_sum = jnp.einsum(
        "bhp,bphd->bhd",
        local_probs.astype(jnp.bfloat16),
        value_block,
        preferred_element_type=jnp.float32,
    ).astype(jnp.bfloat16)
    initial = (
        jnp.full((batch_rows, heads_here), MASKED, jnp.float32),
        jnp.zeros((batch_rows, heads_here), jnp.float32),
        jnp.zeros((batch_rows, heads_here, HEAD_DIM), jnp.float32),
    )
    run_top, run_mass, run_sum = absorb_parts(
        initial,
        (
            lax.all_gather(local_top[None].astype(jnp.bfloat16), "tp", axis=0, tiled=True).astype(
                jnp.float32
            ),
            lax.all_gather(local_mass[None].astype(jnp.bfloat16), "tp", axis=0, tiled=True).astype(
                jnp.float32
            ),
            lax.all_gather(local_sum[None], "tp", axis=0, tiled=True),
        ),
    )
    new_heads = key_new.reshape(batch_rows, heads_here, HEAD_DIM).astype(jnp.float32)
    own_score = jnp.sum(query_heads.astype(jnp.float32) * new_heads, axis=2) * HEAD_DIM ** (-0.5)
    highest = jnp.maximum(run_top, own_score)
    rescale = jnp.exp(run_top - highest)
    own_weight = jnp.exp(own_score - highest)
    own_values = value_new.reshape(batch_rows, heads_here, HEAD_DIM).astype(jnp.float32)
    numer = run_sum * rescale[:, :, None] + own_weight[:, :, None] * own_values
    denom = run_mass * rescale + own_weight
    return (
        (numer / denom[:, :, None]).astype(jnp.bfloat16).reshape(batch_rows, heads_here * HEAD_DIM)
    )


def on_device(
    tokens,
    pre_gain,
    gate_first,
    up_first,
    down_first,
    mix_gain,
    query_w,
    key_w,
    value_w,
    forget_w,
    key_cache,
    value_cache,
    gate_cache,
    lengths,
    out_w,
    post_gain,
    gate_second,
    up_second,
    down_second,
):
    after_first = half_step(tokens, pre_gain, gate_first, up_first, down_first)
    attended = attention(
        after_first,
        mix_gain,
        query_w,
        key_w,
        value_w,
        forget_w,
        key_cache,
        value_cache,
        gate_cache,
        lengths,
    )
    projected = lax.psum(jnp.dot(attended, out_w, preferred_element_type=jnp.float32), "kv")
    residual_two = (after_first.astype(jnp.float32) + projected).astype(jnp.bfloat16)
    return half_step(residual_two, post_gain, gate_second, up_second, down_second)


def solution(mesh):
    placed = (
        P("grp", "tp"),
        P("tp"),
        P("tp", "kv"),
        P("tp", "kv"),
        P("kv", "tp"),
        P("tp"),
        P("tp", "kv"),
        P("tp", "kv"),
        P("tp", "kv"),
        P("tp", None),
        P("grp", "tp", "kv"),
        P("grp", "tp", "kv"),
        P("grp", "kv", "tp"),
        P("grp"),
        P("kv", "tp"),
        P("tp"),
        P("tp", "kv"),
        P("tp", "kv"),
        P("kv", "tp"),
    )
    return jax.shard_map(
        on_device, mesh=mesh, in_specs=placed, out_specs=P("grp", "tp"), check_vma=False
    )
```

profile of v0, /device:TPU:0, one launch (start us, length us, event | category | flops | bytes accessed | tf_op | source)
XLA Modules:
  0.0 220.3 jit_solution(18089456365356496139)
XLA Ops:
  6.5 0.0 copy-start.1
  6.6 1.5 fusion.15
  8.1 4.5 %convolution_convert_fusion.3 = bf16[8,2816]{1,0:T(8,128)(2,1)} fusion(bf16[1024,2816]{1,0:T(8,128)(2,1)} %param.21, bf16[8,1024]{1,0:T(8,128)(2,1)} %param.19, f32[1024]{0:T(1024)} %param.20), kind=kOutput, calls=%fused_computation.6 | convolution fusion | flops 46184448 | bytes 5832704 | tf_op jit(solution)/shard_map/dot_general | solution.py:16
  12.6 1.5 convolution_convert_fusion.2
  14.1 0.0 all-reduce.11.cloned.1.call-update
  14.1 0.0 all-reduce.7.cloned.1.call-start
  14.1 33.9 %all-reduce.11.cloned.1.call-done = (bf16[8,2816]{1,0:T(8,128)(2,1)}, bf16[8,2816]{1,0:T(8,128)(2,1)}, bf16[8]{0:T(256)(128)(2,1)}) async-done(((bf16[8,2816]{1,0:T(8,128)(2,1)}, bf16[8,2816]{1,0:T(8,128)(2,1)}, bf16[8]{0:T(256)(128)(2,1)}), (bf16[8,2816]{1,0:T(8,128)(2,1)}, bf16[8,2816]{1,0:T(8,128)(2,1)}, bf16[8]{0:T(256)(128)(2,1)})) %all-reduce.11.cloned.1.call-update) | async-done | bytes 90144 | tf_op jit(solution)/shard_map/psum | solution.py:20
  48.1 0.7 add_rsqrt_fusion.2
  48.7 3.6 %fusion.9 = f32[8,1024]{1,0:T(8,128)S(1)} fusion(bf16[2816,1024]{1,0:T(8,128)(2,1)} %param.23, bf16[8,2816]{1,0:T(8,128)(2,1)} %get-tuple-element.13, bf16[8,2816]{1,0:T(8,128)(2,1)} %get-tuple-element.14, f32[8]{0:T(128)S(1)} %add_rsqrt_fusion.2), kind=kOutput, calls=%fused_computation.28 | convolution fusion | flops 46362624 | bytes 5890080 | tf_op jit(solution)/shard_map/dot_general | solution.py:25
  52.3 19.1 %psum.101 = f32[8,1024]{1,0:T(8,128)S(1)} all-reduce(f32[8,1024]{1,0:T(8,128)S(1)} %fusion.9), channel_id=1, replica_groups=mesh['grp'=2,'kv'=4,'tp'=4] {'kv'}, use_global_device_ids=true, to_apply=%region_4.5 | all-reduce | flops 8192 | bytes 65536 | tf_op jit(solution)/shard_map/psum | solution.py:26
  71.4 0.0 copy-start.3
  71.4 0.7 fusion.18
  72.2 0.7 fusion.45
  72.9 1.0 fusion.43
  73.9 2.6 %fusion.41 = f32[8,1024]{1,0:T(8,128)} fusion(bf16[1024,1024]{1,0:T(8,128)(2,1)} %param.27, bf16[8,1024]{1,0:T(8,128)(2,1)S(1)} %get-tuple-element.21, f32[1024]{0:T(1024)S(1)} %copy-done.5), kind=kOutput, calls=%fused_computation.68 | convolution fusion | flops 16801792 | bytes 2150400 | tf_op jit(solution)/shard_map/dot_general | solution.py:60
  76.4 1.0 fusion.47
  77.4 0.0 all-reduce.7.cloned.1.call-update
  77.5 0.0 all-reduce.9.cloned.1.call-start
  77.5 0.1 broadcast_compare_fusion
  77.6 6.4 %copy.38 = bf16[8,256,1024]{1,2,0:T(8,128)(2,1)} copy(bf16[8,256,1024]{2,1,0:T(8,128)(2,1)} %param.29) | data formatting | bytes 8388608 | tf_op jit(solution)/shard_map/reshape | solution.py:77
  84.0 21.8 %all-reduce.7.cloned.1.call-done = (f32[8,1024]{1,0:T(8,128)}, f32[8]{0:T(128)}, f32[8,32]{1,0:T(8,128)}, f32[8,1024]{1,0:T(8,128)}, f32[8,1024]{1,0:T(8,128)}) async-done(((f32[8,1024]{1,0:T(8,128)}, f32[8]{0:T(128)}, f32[8,32]{1,0:T(8,128)}, f32[8,1024]{1,0:T(8,128)}, f32[8,1024]{1,0:T(8,128)}), (f32[8,1024]{1,0:T(8,128)}, f32[8]{0:T(128)}, f32[8,32]{1,0:T(8,128)}, f32[8,1024]{1,0:T(8,128)}, ...) | async-done | bytes 99376 | tf_op jit(solution)/shard_map/psum | solution.py:62
  105.8 0.7 add_rsqrt_fusion.1
  106.5 0.8 fusion.54
  107.4 0.9 fusion.27
  108.3 0.1 copy.29
  108.4 0.8 fusion.51
  109.1 2.8 %fusion.28 = f32[8,8,1,256]{3,2,1,0:T(1,128)S(1)} fusion(bf16[8,256,8,128]{1,3,2,0:T(8,128)(2,1)} %bitcast.68, bf16[8,8,128,1]{2,0,1,3:T(8,128)(2,1)S(1)} %fusion.54), kind=kOutput, calls=%fused_computation.50 | convolution fusion | flops 4194304 | bytes 4276224 | tf_op jit(solution)/shard_map/bhd,bphd->bhp/dot_general | solution.py:79
  112.0 0.2 select_reduce_fusion
  112.2 0.2 fusion.7
  112.3 5.2 %all-gather = bf16[32,8]{1,0:T(8,128)(2,1)S(1)} all-gather(bf16[8,8]{1,0:T(8,128)(2,1)S(1)} %convert_element_type.152), channel_id=2, replica_groups=mesh['grp'=2,'kv'=4,'tp'=4] {'tp'}, dimensions={0}, use_global_device_ids=true | all-gather | bytes 640 | tf_op jit(solution)/shard_map/all_gather | solution.py:102
  117.6 5.5 %all-gather.2 = bf16[32,8]{1,0:T(8,128)(2,1)S(1)} all-gather(bf16[8,8]{1,0:T(8,128)(2,1)S(1)} %get-tuple-element.22), channel_id=4, replica_groups=mesh['grp'=2,'kv'=4,'tp'=4] {'tp'}, dimensions={0}, use_global_device_ids=true | all-gather | bytes 640 | tf_op jit(solution)/shard_map/all_gather | solution.py:105
  123.1 0.1 copy.30
  123.2 0.1 copy.31
  123.2 3.0 %fusion = f32[8,8,1,128]{3,2,1,0:T(1,128)S(1)} fusion(bf16[8,8,256,1]{2,1,0,3:T(8,128)(2,1)S(1)} %get-tuple-element.23, bf16[8,256,1024]{2,1,0:T(8,128)(2,1)} %param.30), kind=kOutput, calls=%fused_computation | convolution fusion | flops 4194304 | bytes 4259840 | tf_op jit(solution)/shard_map/bhp,bphd->bhd/dot_general | solution.py:88
  126.2 5.2 %all-gather.1 = bf16[32,8,128]{2,1,0:T(8,128)(2,1)S(1)} all-gather(bf16[8,8,128]{2,1,0:T(8,128)(2,1)S(1)} %convert_element_type.155), channel_id=3, replica_groups=mesh['grp'=2,'kv'=4,'tp'=4] {'tp'}, dimensions={0}, use_global_device_ids=true | all-gather | bytes 81920 | tf_op jit(solution)/shard_map/all_gather | solution.py:108
  131.5 0.1 fusion.3
  131.6 0.1 multiply_bitcast_fusion
  131.7 0.4 fusion.31
  132.1 19.3 %psum.107 = f32[8,1024]{1,0:T(8,128)S(1)} all-reduce(f32[8,1024]{1,0:T(8,128)S(1)} %fusion.31), channel_id=1, replica_groups=mesh['grp'=2,'kv'=4,'tp'=4] {'kv'}, use_global_device_ids=true, to_apply=%region_17.18 | all-reduce | flops 8192 | bytes 65536 | tf_op jit(solution)/shard_map/psum | solution.py:158
  151.4 0.6 fusion.21
  152.1 4.1 %convolution_convert_fusion.1 = bf16[8,2816]{1,0:T(8,128)(2,1)} fusion(bf16[1024,2816]{1,0:T(8,128)(2,1)} %param.35, bf16[8,1024]{1,0:T(8,128)(2,1)S(1)} %get-tuple-element.17, f32[1024]{0:T(1024)S(1)} %copy-done.10), kind=kOutput, calls=%fused_computation.4 | convolution fusion | flops 46184448 | bytes 5832704 | tf_op jit(solution)/shard_map/dot_general | solution.py:16
  156.2 4.1 %convolution_convert_fusion = bf16[8,2816]{1,0:T(8,128)(2,1)} fusion(bf16[1024,2816]{1,0:T(8,128)(2,1)} %param.36, bf16[8,1024]{1,0:T(8,128)(2,1)S(1)} %get-tuple-element.17, f32[1024]{0:T(1024)S(1)} %copy-done.10), kind=kOutput, calls=%fused_computation.3 | convolution fusion | flops 46184448 | bytes 5832704 | tf_op jit(solution)/shard_map/dot_general | solution.py:17
  160.3 0.0 all-reduce.9.cloned.1.call-update
  160.3 29.6 %all-reduce.9.cloned.1.call-done = (bf16[8,2816]{1,0:T(8,128)(2,1)}, bf16[8,2816]{1,0:T(8,128)(2,1)}, bf16[8]{0:T(256)(128)(2,1)}) async-done(((bf16[8,2816]{1,0:T(8,128)(2,1)}, bf16[8,2816]{1,0:T(8,128)(2,1)}, bf16[8]{0:T(256)(128)(2,1)}), (bf16[8,2816]{1,0:T(8,128)(2,1)}, bf16[8,2816]{1,0:T(8,128)(2,1)}, bf16[8]{0:T(256)(128)(2,1)})) %all-reduce.9.cloned.1.call-update) | async-done | bytes 90144 | tf_op jit(solution)/shard_map/psum | solution.py:20
  190.0 0.7 add_rsqrt_fusion
  190.6 3.6 %fusion.10 = f32[8,1024]{1,0:T(8,128)S(1)} fusion(bf16[2816,1024]{1,0:T(8,128)(2,1)} %param.37, bf16[8,2816]{1,0:T(8,128)(2,1)} %get-tuple-element.10, bf16[8,2816]{1,0:T(8,128)(2,1)} %get-tuple-element.11, f32[8]{0:T(128)S(1)} %add_rsqrt_fusion), kind=kOutput, calls=%fused_computation.29 | convolution fusion | flops 46362624 | bytes 5890080 | tf_op jit(solution)/shard_map/dot_general | solution.py:25
  194.2 19.0 %psum.111 = f32[8,1024]{1,0:T(8,128)S(1)} all-reduce(f32[8,1024]{1,0:T(8,128)S(1)} %fusion.10), channel_id=1, replica_groups=mesh['grp'=2,'kv'=4,'tp'=4] {'kv'}, use_global_device_ids=true, to_apply=%region_22.23 | all-reduce | flops 8192 | bytes 65536 | tf_op jit(solution)/shard_map/psum | solution.py:26
  213.2 0.6 fusion.23
  (30 shorter events, 0.1 us)
Async XLA Ops:
  6.5 66.3 %copy-start = (bf16[1024,1024]{1,0:T(8,128)(2,1)S(1)}, bf16[1024,1024]{1,0:T(8,128)(2,1)}, u32[]{:S(2)}) copy-start(bf16[1024,1024]{1,0:T(8,128)(2,1)} %param.26) | copy-start | bytes 6291460
  6.5 6.0 %copy-start.4 = (bf16[8,1024]{1,0:T(8,128)(2,1)S(1)}, bf16[8,1024]{1,0:T(8,128)(2,1)}, u32[]{:S(2)}) copy-start(bf16[8,1024]{1,0:T(8,128)(2,1)} %param.19) | copy-start | bytes 49156
  6.5 6.0 %copy-start.9 = (f32[1024]{0:T(1024)S(1)}, f32[1024]{0:T(1024)}, u32[]{:S(2)}) copy-start(f32[1024]{0:T(1024)} %param.20) | copy-start | bytes 12292
  6.5 41.5 %all-reduce.11.cloned.1.call-start = ((), (), s32[]{:S(2)}) async-start(), calls=%async_computation.2 | async-start | bytes 181248 | tf_op jit(solution)/shard_map/psum | solution.py:20
  6.5 6.0 %copy-start.1 = (bf16[1024,2816]{1,0:T(8,128)(2,1)S(1)}, bf16[1024,2816]{1,0:T(8,128)(2,1)}, u32[]{:S(2)}) copy-start(bf16[1024,2816]{1,0:T(8,128)(2,1)} %param.22) | copy-start | bytes 17301508
  14.0 58.1 %copy-start.5 = (f32[1024]{0:T(1024)S(1)}, f32[1024]{0:T(1024)}, u32[]{:S(2)}) copy-start(f32[1024]{0:T(1024)} %param.24) | copy-start | bytes 12292
  14.0 58.1 %copy-start.7 = (bf16[1024,32]{0,1:T(8,128)(2,1)S(1)}, bf16[1024,32]{0,1:T(8,128)(2,1)}, u32[]{:S(2)}) copy-start(bf16[1024,32]{0,1:T(8,128)(2,1)} %param.28) | copy-start | bytes 196612
  14.1 91.8 %all-reduce.7.cloned.1.call-start = ((), (), s32[]{:S(2)}) async-start(), calls=%async_computation | async-start | bytes 205824 | tf_op jit(solution)/shard_map/psum | solution.py:62
  52.3 25.2 %copy-start.11 = (s32[8]{0:T(128)S(1)}, s32[8]{0:T(128)}, u32[]{:S(2)}) copy-start(s32[8]{0:T(128)} %param.32) | copy-start | bytes 100
  71.4 5.0 %copy-start.3 = (bf16[1024,1024]{1,0:T(8,128)(2,1)S(1)}, bf16[1024,1024]{1,0:T(8,128)(2,1)}, u32[]{:S(2)}) copy-start(bf16[1024,1024]{1,0:T(8,128)(2,1)} %param.25) | copy-start | bytes 6291460
  77.5 112.5 %all-reduce.9.cloned.1.call-start = ((), (), s32[]{:S(2)}) async-start(), calls=%async_computation.1 | async-start | bytes 181248 | tf_op jit(solution)/shard_map/psum | solution.py:20
  84.0 28.0 %copy-start.6 = (f32[8,8,256]{2,1,0:T(8,128)S(1)}, f32[8,8,256]{2,1,0:T(8,128)}, u32[]{:S(2)}) copy-start(f32[8,8,256]{2,1,0:T(8,128)} %param.31) | copy-start | bytes 196612
  109.1 22.5 %copy-start.8 = (f32[8,1024]{1,0:T(8,128)S(1)}, f32[8,1024]{1,0:T(8,128)}, u32[]{:S(2)}) copy-start(f32[8,1024]{1,0:T(8,128)} %get-tuple-element.9) | copy-start | bytes 98308
  112.0 40.1 %copy-start.10 = (f32[1024]{0:T(1024)S(1)}, f32[1024]{0:T(1024)}, u32[]{:S(2)}) copy-start(f32[1024]{0:T(1024)} %param.34) | copy-start | bytes 12292
  123.2 8.4 %copy-start.2 = (bf16[1024,1024]{1,0:T(8,128)(2,1)S(1)}, bf16[1024,1024]{1,0:T(8,128)(2,1)}, u32[]{:S(2)}) copy-start(bf16[1024,1024]{1,0:T(8,128)(2,1)} %param.33) | copy-start | bytes 6291460
Sparse Core Ops, SparseCore 0:
  14.2 33.8 all-reduce.10
  77.6 28.2 all-reduce.6
  160.4 29.4 all-reduce.8
where the time goes:
time: 221 us; the launch traced here: 220 us
  waiting for transfers between devices  85.4 us (39%)
  blocking collectives  73.4 us (33%)
  matrix products  32.9 us (15%)
  between operations  13.3 us (6%)
  other arithmetic  8.63 us (4%)
  local copies, waits for them, and re-layouts  6.69 us (3%)
    psum x2, waiting for transfers between devices, half_step(): lax.psum(up_part.astype(jnp.bfloat16), 'tp').astype(jnp.float32)  63.5 us
    psum x2, blocking collectives, half_step(): down_sum = lax.psum(down_part, 'kv')  38.1 us
    psum x1, waiting for transfers between devices, attention(): lax.psum((query_part, key_part, value_part, forget_part, squares), 'tp')  21.8 us
    psum x1, blocking collectives, on_device(): lax.psum(jnp.dot(attended, out_w, preferred_element_type=jnp.float32), 'kv')  19.3 us
    dot_general x2, matrix products, half_step(): gate_part = jnp.dot(weighted, w_gate, preferred_element_type=jnp.float32)  8.61 us
    dot_general x2, matrix products, half_step(): down_part = jnp.dot(hidden, w_down, preferred_element_type=jnp.float32)  7.18 us
    reshape x1, local copies, waits for them, and re-layouts, attention(): key_block = key_cache.reshape(batch_rows, cache_span, heads_here, HEAD_DIM)  6.44 us
    dot_general x2, matrix products, half_step(): up_part = jnp.dot(weighted, w_up, preferred_element_type=jnp.float32)  5.58 us
  transfers between devices with their start and end apart: 3, of which 3 were waited for; matrix products, arithmetic and copies ran while one was open for 3% of the time, Pallas kernels for 0%

commit v1 on v0

--- a/solution.py
+++ b/solution.py
@@ -23,7 +23,8 @@
     norm_scale = lax.rsqrt(sq_total / D + EPSILON)[:, None]
     hidden = (jax.nn.silu(norm_scale * gate_sum) * (norm_scale * up_sum)).astype(jnp.bfloat16)
     down_part = jnp.dot(hidden, w_down, preferred_element_type=jnp.float32)
-    down_sum = lax.psum(down_part, "kv")
+    fix_lots_all = lambda mine_x, axis_name: jnp.sum(lax.all_gather(mine_x, axis_name), 0)
+    down_sum = fix_lots_all(down_part, axis_name="kv")
     return (widened + 0.5 * down_sum).astype(jnp.bfloat16)
 
 

time: 221 us -> 211 us (0.955)
  blocking collectives: 73.4 us -> 62.2 us
  waiting for transfers between devices: 85.4 us -> 88.1 us
    psum x2 -> x0, blocking collectives: 38.1 us -> none  [half_step(): down_sum = lax.psum(down_part, 'kv')]
    all_gather x0 -> x2, blocking collectives: none -> 26.9 us  [half_step(): lax.all_gather(mine_x, axis_name)]
    psum x1, waiting for transfers between devices: 21.8 us -> 24.5 us  [attention(): lax.psum((query_part, key_part, value_part, forget_part, squares), 'tp')]
where the time goes in v1:
time: 211 us; the launch traced here: 210 us
  waiting for transfers between devices  88.1 us (42%)
  blocking collectives  62.2 us (29%)
  matrix products  31.5 us (15%)
  between operations  13.2 us (6%)
  other arithmetic  8.65 us (4%)
  local copies, waits for them, and re-layouts  6.69 us (3%)
    psum x2, waiting for transfers between devices, half_step(): lax.psum(up_part.astype(jnp.bfloat16), 'tp').astype(jnp.float32)  63.5 us
    all_gather x2, blocking collectives, half_step(): lax.all_gather(mine_x, axis_name)  26.9 us
    psum x1, waiting for transfers between devices, attention(): lax.psum((query_part, key_part, value_part, forget_part, squares), 'tp')  24.5 us
    psum x1, blocking collectives, on_device(): lax.psum(jnp.dot(attended, out_w, preferred_element_type=jnp.float32), 'kv')  19.3 us
    dot_general x2, matrix products, half_step(): gate_part = jnp.dot(weighted, w_gate, preferred_element_type=jnp.float32)  8.61 us
    dot_general x2, matrix products, half_step(): down_part = jnp.dot(hidden, w_down, preferred_element_type=jnp.float32)  7.33 us
    reshape x1, local copies, waits for them, and re-layouts, attention(): key_block = key_cache.reshape(batch_rows, cache_span, heads_here, HEAD_DIM)  6.43 us
    dot_general x2, matrix products, half_step(): up_part = jnp.dot(weighted, w_up, preferred_element_type=jnp.float32)  5.58 us
  transfers between devices with their start and end apart: 3, of which 3 were waited for; matrix products, arithmetic and copies ran while one was open for 3% of the time, Pallas kernels for 0%

profile of v1, /device:TPU:0, one launch (start us, length us, event | category | flops | bytes accessed | tf_op | source)
XLA Modules:
  0.0 210.5 jit_solution(5156036471447752741)
XLA Ops:
  6.5 0.0 copy-start.1
  6.6 1.5 fusion.15
  8.1 4.5 %convolution_convert_fusion.3 = bf16[8,2816]{1,0:T(8,128)(2,1)} fusion(bf16[1024,2816]{1,0:T(8,128)(2,1)} %param.21, bf16[8,1024]{1,0:T(8,128)(2,1)} %param.19, f32[1024]{0:T(1024)} %param.20), kind=kOutput, calls=%fused_computation.6 | convolution fusion | flops 46184448 | bytes 5832704 | tf_op jit(solution)/shard_map/dot_general | solution.py:16
  12.6 0.0 copy-done.10
  12.6 1.5 convolution_convert_fusion.2
  14.1 0.0 all-reduce.11.cloned.1.call-update
  14.1 0.0 all-reduce.7.cloned.1.call-start
  14.1 33.9 %all-reduce.11.cloned.1.call-done = (bf16[8,2816]{1,0:T(8,128)(2,1)}, bf16[8,2816]{1,0:T(8,128)(2,1)}, bf16[8]{0:T(256)(128)(2,1)}) async-done(((bf16[8,2816]{1,0:T(8,128)(2,1)}, bf16[8,2816]{1,0:T(8,128)(2,1)}, bf16[8]{0:T(256)(128)(2,1)}), (bf16[8,2816]{1,0:T(8,128)(2,1)}, bf16[8,2816]{1,0:T(8,128)(2,1)}, bf16[8]{0:T(256)(128)(2,1)})) %all-reduce.11.cloned.1.call-update) | async-done | bytes 90144 | tf_op jit(solution)/shard_map/psum | solution.py:20
  48.1 0.7 add_rsqrt_fusion.2
  48.7 3.7 %fusion.9 = f32[8,1024]{1,0:T(8,128)S(1)} fusion(bf16[2816,1024]{1,0:T(8,128)(2,1)} %param.23, bf16[8,2816]{1,0:T(8,128)(2,1)} %get-tuple-element.13, bf16[8,2816]{1,0:T(8,128)(2,1)} %get-tuple-element.14, f32[8]{0:T(128)S(1)} %add_rsqrt_fusion.2), kind=kOutput, calls=%fused_computation.30 | convolution fusion | flops 46362624 | bytes 5890080 | tf_op jit(solution)/shard_map/dot_general | solution.py:25
  52.5 13.5 %all-gather = f32[32,1024]{1,0:T(8,128)S(1)} all-gather(f32[8,1024]{1,0:T(8,128)S(1)} %fusion.9), channel_id=2, replica_groups=mesh['grp'=2,'kv'=4,'tp'=4] {'kv'}, dimensions={0}, use_global_device_ids=true | all-gather | bytes 163840 | tf_op jit(solution)/shard_map/all_gather | solution.py:26
  66.0 0.7 fusion.18
  66.7 0.7 fusion.45
  67.4 1.0 fusion.43
  68.4 1.0 fusion.41
  69.4 1.0 fusion.47
  70.4 0.0 all-reduce.7.cloned.1.call-update
  70.4 0.0 all-reduce.9.cloned.1.call-start
  70.5 0.1 broadcast_compare_fusion
  70.6 6.4 %copy.38 = bf16[8,256,1024]{1,2,0:T(8,128)(2,1)} copy(bf16[8,256,1024]{2,1,0:T(8,128)(2,1)} %param.29) | data formatting | bytes 8388608 | tf_op jit(solution)/shard_map/reshape | solution.py:78
  77.0 24.5 %all-reduce.7.cloned.1.call-done = (f32[8,1024]{1,0:T(8,128)}, f32[8]{0:T(128)}, f32[8,32]{1,0:T(8,128)}, f32[8,1024]{1,0:T(8,128)}, f32[8,1024]{1,0:T(8,128)}) async-done(((f32[8,1024]{1,0:T(8,128)}, f32[8]{0:T(128)}, f32[8,32]{1,0:T(8,128)}, f32[8,1024]{1,0:T(8,128)}, f32[8,1024]{1,0:T(8,128)}), (f32[8,1024]{1,0:T(8,128)}, f32[8]{0:T(128)}, f32[8,32]{1,0:T(8,128)}, f32[8,1024]{1,0:T(8,128)}, ...) | async-done | bytes 99376 | tf_op jit(solution)/shard_map/psum | solution.py:63
  101.5 0.7 add_rsqrt_fusion.1
  102.2 0.8 fusion.54
  103.1 0.9 fusion.27
  104.0 0.1 copy.29
  104.1 0.8 fusion.51
  104.8 2.8 %fusion.28 = f32[8,8,1,256]{3,2,1,0:T(1,128)S(1)} fusion(bf16[8,256,8,128]{1,3,2,0:T(8,128)(2,1)} %bitcast.72, bf16[8,8,128,1]{2,0,1,3:T(8,128)(2,1)S(1)} %fusion.54), kind=kOutput, calls=%fused_computation.52 | convolution fusion | flops 4194304 | bytes 4276224 | tf_op jit(solution)/shard_map/bhd,bphd->bhp/dot_general | solution.py:80
  107.7 0.2 select_reduce_fusion
  107.9 0.2 fusion.7
  108.0 5.2 %all-gather.1 = bf16[32,8]{1,0:T(8,128)(2,1)S(1)} all-gather(bf16[8,8]{1,0:T(8,128)(2,1)S(1)} %convert_element_type.152), channel_id=3, replica_groups=mesh['grp'=2,'kv'=4,'tp'=4] {'tp'}, dimensions={0}, use_global_device_ids=true | all-gather | bytes 640 | tf_op jit(solution)/shard_map/all_gather | solution.py:103
  113.3 5.5 %all-gather.3 = bf16[32,8]{1,0:T(8,128)(2,1)S(1)} all-gather(bf16[8,8]{1,0:T(8,128)(2,1)S(1)} %get-tuple-element.22), channel_id=5, replica_groups=mesh['grp'=2,'kv'=4,'tp'=4] {'tp'}, dimensions={0}, use_global_device_ids=true | all-gather | bytes 640 | tf_op jit(solution)/shard_map/all_gather | solution.py:106
  118.8 0.1 copy.30
  118.9 0.1 copy.31
  118.9 3.0 %fusion = f32[8,8,1,128]{3,2,1,0:T(1,128)S(1)} fusion(bf16[8,8,256,1]{2,1,0,3:T(8,128)(2,1)S(1)} %get-tuple-element.23, bf16[8,256,1024]{2,1,0:T(8,128)(2,1)} %param.30), kind=kOutput, calls=%fused_computation | convolution fusion | flops 4194304 | bytes 4259840 | tf_op jit(solution)/shard_map/bhp,bphd->bhd/dot_general | solution.py:89
  121.9 5.2 %all-gather.2 = bf16[32,8,128]{2,1,0:T(8,128)(2,1)S(1)} all-gather(bf16[8,8,128]{2,1,0:T(8,128)(2,1)S(1)} %convert_element_type.155), channel_id=4, replica_groups=mesh['grp'=2,'kv'=4,'tp'=4] {'tp'}, dimensions={0}, use_global_device_ids=true | all-gather | bytes 81920 | tf_op jit(solution)/shard_map/all_gather | solution.py:109
  127.2 0.1 fusion.3
  127.3 0.1 multiply_bitcast_fusion
  127.4 0.4 fusion.31
  127.8 19.3 %psum.92 = f32[8,1024]{1,0:T(8,128)S(1)} all-reduce(f32[8,1024]{1,0:T(8,128)S(1)} %fusion.31), channel_id=1, replica_groups=mesh['grp'=2,'kv'=4,'tp'=4] {'kv'}, use_global_device_ids=true, to_apply=%region_17.18 | all-reduce | flops 8192 | bytes 65536 | tf_op jit(solution)/shard_map/psum | solution.py:159
  147.2 0.6 fusion.21
  147.8 4.1 %convolution_convert_fusion.1 = bf16[8,2816]{1,0:T(8,128)(2,1)} fusion(bf16[1024,2816]{1,0:T(8,128)(2,1)} %param.35, bf16[8,1024]{1,0:T(8,128)(2,1)S(1)} %get-tuple-element.17, f32[1024]{0:T(1024)S(1)} %copy-done.11), kind=kOutput, calls=%fused_computation.4 | convolution fusion | flops 46184448 | bytes 5832704 | tf_op jit(solution)/shard_map/dot_general | solution.py:16
  151.9 4.1 %convolution_convert_fusion = bf16[8,2816]{1,0:T(8,128)(2,1)} fusion(bf16[1024,2816]{1,0:T(8,128)(2,1)} %param.36, bf16[8,1024]{1,0:T(8,128)(2,1)S(1)} %get-tuple-element.17, f32[1024]{0:T(1024)S(1)} %copy-done.11), kind=kOutput, calls=%fused_computation.3 | convolution fusion | flops 46184448 | bytes 5832704 | tf_op jit(solution)/shard_map/dot_general | solution.py:17
  156.0 0.0 all-reduce.9.cloned.1.call-update
  156.0 29.6 %all-reduce.9.cloned.1.call-done = (bf16[8,2816]{1,0:T(8,128)(2,1)}, bf16[8,2816]{1,0:T(8,128)(2,1)}, bf16[8]{0:T(256)(128)(2,1)}) async-done(((bf16[8,2816]{1,0:T(8,128)(2,1)}, bf16[8,2816]{1,0:T(8,128)(2,1)}, bf16[8]{0:T(256)(128)(2,1)}), (bf16[8,2816]{1,0:T(8,128)(2,1)}, bf16[8,2816]{1,0:T(8,128)(2,1)}, bf16[8]{0:T(256)(128)(2,1)})) %all-reduce.9.cloned.1.call-update) | async-done | bytes 90144 | tf_op jit(solution)/shard_map/psum | solution.py:20
  185.7 0.7 add_rsqrt_fusion
  186.3 3.6 %fusion.10 = f32[8,1024]{1,0:T(8,128)S(1)} fusion(bf16[2816,1024]{1,0:T(8,128)(2,1)} %param.37, bf16[8,2816]{1,0:T(8,128)(2,1)} %get-tuple-element.10, bf16[8,2816]{1,0:T(8,128)(2,1)} %get-tuple-element.11, f32[8]{0:T(128)S(1)} %add_rsqrt_fusion), kind=kOutput, calls=%fused_computation.31 | convolution fusion | flops 46362624 | bytes 5890080 | tf_op jit(solution)/shard_map/dot_general | solution.py:25
  189.9 13.4 %all-gather.4 = f32[32,1024]{1,0:T(8,128)S(1)} all-gather(f32[8,1024]{1,0:T(8,128)S(1)} %fusion.10), channel_id=6, replica_groups=mesh['grp'=2,'kv'=4,'tp'=4] {'kv'}, dimensions={0}, use_global_device_ids=true | all-gather | bytes 163840 | tf_op jit(solution)/shard_map/all_gather | solution.py:26
  203.3 0.6 fusion.23
  (34 shorter events, 0.1 us)
Async XLA Ops:
  6.5 60.9 %copy-start = (bf16[1024,1024]{1,0:T(8,128)(2,1)S(1)}, bf16[1024,1024]{1,0:T(8,128)(2,1)}, u32[]{:S(2)}) copy-start(bf16[1024,1024]{1,0:T(8,128)(2,1)} %param.26) | copy-start | bytes 6291460
  6.5 6.0 %copy-start.5 = (bf16[8,1024]{1,0:T(8,128)(2,1)S(1)}, bf16[8,1024]{1,0:T(8,128)(2,1)}, u32[]{:S(2)}) copy-start(bf16[8,1024]{1,0:T(8,128)(2,1)} %param.19) | copy-start | bytes 49156
  6.5 6.0 %copy-start.10 = (f32[1024]{0:T(1024)S(1)}, f32[1024]{0:T(1024)}, u32[]{:S(2)}) copy-start(f32[1024]{0:T(1024)} %param.20) | copy-start | bytes 12292
  6.5 41.5 %all-reduce.11.cloned.1.call-start = ((), (), s32[]{:S(2)}) async-start(), calls=%async_computation.2 | async-start | bytes 181248 | tf_op jit(solution)/shard_map/psum | solution.py:20
  6.5 6.0 %copy-start.1 = (bf16[1024,2816]{1,0:T(8,128)(2,1)S(1)}, bf16[1024,2816]{1,0:T(8,128)(2,1)}, u32[]{:S(2)}) copy-start(bf16[1024,2816]{1,0:T(8,128)(2,1)} %param.22) | copy-start | bytes 17301508
  14.0 52.7 %copy-start.6 = (f32[1024]{0:T(1024)S(1)}, f32[1024]{0:T(1024)}, u32[]{:S(2)}) copy-start(f32[1024]{0:T(1024)} %param.24) | copy-start | bytes 12292
  14.0 52.7 %copy-start.8 = (bf16[1024,32]{0,1:T(8,128)(2,1)S(1)}, bf16[1024,32]{0,1:T(8,128)(2,1)}, u32[]{:S(2)}) copy-start(bf16[1024,32]{0,1:T(8,128)(2,1)} %param.28) | copy-start | bytes 196612
  14.1 87.5 %all-reduce.7.cloned.1.call-start = ((), (), s32[]{:S(2)}) async-start(), calls=%async_computation | async-start | bytes 205824 | tf_op jit(solution)/shard_map/psum | solution.py:63
  48.7 19.7 %copy-start.3 = (bf16[1024,1024]{1,0:T(8,128)(2,1)S(1)}, bf16[1024,1024]{1,0:T(8,128)(2,1)}, u32[]{:S(2)}) copy-start(bf16[1024,1024]{1,0:T(8,128)(2,1)} %param.27) | copy-start | bytes 6291460
  48.7 20.7 %copy-start.4 = (bf16[1024,1024]{1,0:T(8,128)(2,1)S(1)}, bf16[1024,1024]{1,0:T(8,128)(2,1)}, u32[]{:S(2)}) copy-start(bf16[1024,1024]{1,0:T(8,128)(2,1)} %param.25) | copy-start | bytes 6291460
  52.5 18.0 %copy-start.12 = (s32[8]{0:T(128)S(1)}, s32[8]{0:T(128)}, u32[]{:S(2)}) copy-start(s32[8]{0:T(128)} %param.32) | copy-start | bytes 100
  70.4 115.2 %all-reduce.9.cloned.1.call-start = ((), (), s32[]{:S(2)}) async-start(), calls=%async_computation.1 | async-start | bytes 181248 | tf_op jit(solution)/shard_map/psum | solution.py:20
  77.0 30.7 %copy-start.7 = (f32[8,8,256]{2,1,0:T(8,128)S(1)}, f32[8,8,256]{2,1,0:T(8,128)}, u32[]{:S(2)}) copy-start(f32[8,8,256]{2,1,0:T(8,128)} %param.31) | copy-start | bytes 196612
  104.8 22.5 %copy-start.9 = (f32[8,1024]{1,0:T(8,128)S(1)}, f32[8,1024]{1,0:T(8,128)}, u32[]{:S(2)}) copy-start(f32[8,1024]{1,0:T(8,128)} %get-tuple-element.9) | copy-start | bytes 98308
  107.7 40.1 %copy-start.11 = (f32[1024]{0:T(1024)S(1)}, f32[1024]{0:T(1024)}, u32[]{:S(2)}) copy-start(f32[1024]{0:T(1024)} %param.34) | copy-start | bytes 12292
  118.9 8.4 %copy-start.2 = (bf16[1024,1024]{1,0:T(8,128)(2,1)S(1)}, bf16[1024,1024]{1,0:T(8,128)(2,1)}, u32[]{:S(2)}) copy-start(bf16[1024,1024]{1,0:T(8,128)(2,1)} %param.33) | copy-start | bytes 6291460
Sparse Core Ops, SparseCore 0:
  14.2 33.8 all-reduce.10
  70.5 30.9 all-reduce.6
  156.1 29.4 all-reduce.8
